TPU v7x, 32 devices: a whole 2x2x4 slice. The times are simulated.
32 devices in a mesh: grp: 2 (over x), ep: 4 (over y, core), tp: 4 (over z).
Axes of the slice: x: 2, y: 2, z: 4, core: 2. Of those that a mesh axis runs over, the one named last changes fastest.
Arguments:
- pool_input: bfloat16 [8192, 1024], P(('grp', 'ep'), 'tp'), parts along dimension 0, may hold values from -6 to 6
- pool_map: bfloat16 [8, 128, 128], replicated, may hold values from -0.5 to 0.5
- pool_scale: float32 [1024], replicated, may hold values from 0.1 to 1.9
- out_weight: bfloat16 [1024, 2048], P(None, 'tp'), may hold values from -0.1875 to 0.1875
- expert_input: bfloat16 [4096, 2048], P(('grp', 'ep', 'tp')), parts along dimension 0, may hold values from -6 to 6
- norm_gain: float32 [2048], replicated, may hold values from 0.1 to 1.9
- routes: int32 [4096, 2], P(('grp', 'ep', 'tp')), parts along dimension 0, may hold values from 0 to 15, all different within a row; in each aligned block of 128 rows (0 to 127, 128 to 255, ...) at most 32 rows name the same one
- route_weight: float32 [4096, 2], P(('grp', 'ep', 'tp')), parts along dimension 0, may hold values from 0.2 to 1.5
- gate_weight: bfloat16 [16, 2048, 512], P(('ep', 'tp')), may hold values from -0.125 to 0.125
- up_weight: bfloat16 [16, 2048, 512], P(('ep', 'tp')), may hold values from -0.125 to 0.125
- down_weight: bfloat16 [16, 512, 2048], P(('ep', 'tp')), may hold values from -0.25 to 0.25
Outputs:
- pool_output: bfloat16 [8192, 2048], P(('grp', 'ep'), 'tp'), parts along dimension 0
- expert_output: bfloat16 [4096, 2048], P(('grp', 'ep', 'tp')), parts along dimension 0
There are 2 independent parts, one for each index of `grp`. A program takes and returns all parts, laid end to end along the dimension named above; an argument that names none is the same for every part. Nothing has to cross between parts.
Inputs may be any that keep to these rules, and one draw needn't show every extreme that they name: `routes`: each row names 2 different experts. In the rows of one device no expert is named more than 32 times, and in every draw some device names some expert exactly 32 times.
All inputs are finite; a program needn't handle non-finite values.
Results may differ from a plain program's by a relative error of at most 0.007.
Values may be sent and summed in bfloat16 or wider, within the bound.
A program may use at most 64 MiB of HBM per device.

v0:
```python
import jax
import jax.numpy as jnp
from jax import lax
from jax.sharding import PartitionSpec as P

epsilon = 1e-06
halo_depth = 16


def shifted_2(shard, axis, by):
    size = lax.axis_size(axis)
    pairs = [(i, i + by) for i in range(size) if 0 <= i + by < size]
    return lax.ppermute(shard, axis, pairs)


def expert_rows(received, gate_weight, up_weight, down_weight):
    shape_in = received.shape
    flat_rows = received.reshape(-1, shape_in[-1])
    gate_part = jnp.dot(flat_rows, gate_weight[0], preferred_element_type=jnp.float32)
    up_part = jnp.dot(flat_rows, up_weight[0], preferred_element_type=jnp.float32)
    hidden = (jax.nn.silu(gate_part) * up_part).astype(jnp.bfloat16)
    result = jnp.dot(hidden, down_weight[0], preferred_element_type=jnp.float32).astype(
        jnp.bfloat16
    )
    return result.reshape(shape_in)


def pool_half(pool_input, pool_map, pool_scale, out_weight):
    row_count, width_local = pool_input.shape
    group_dim = pool_map.shape[1]
    groups_local = width_local // group_dim
    last_rows = pool_input[row_count - halo_depth :]
    earlier_rows = shifted_2(last_rows, "ep", 1)
    extended = jnp.concatenate([earlier_rows, pool_input], axis=0).astype(jnp.float32)
    first_group = lax.axis_index("tp") * groups_local
    group_ids = first_group + jnp.arange(width_local, dtype=jnp.int32) // group_dim
    window = jnp.left_shift(jnp.int32(2), group_ids % 4)
    summed = jnp.zeros((row_count, width_local), jnp.float32)
    for offset in range(halo_depth):
        shifted = extended[halo_depth - offset : halo_depth - offset + row_count]
        summed = summed + jnp.where(offset < window, shifted, 0.0)
    positions = lax.axis_index("ep") * row_count + jnp.arange(row_count, dtype=jnp.int32)
    counted = jnp.minimum(positions[:, None] + 1, window[None, :]).astype(jnp.float32)
    pooled = (summed / counted - extended[halo_depth:]).astype(jnp.bfloat16)
    maps_local = lax.dynamic_slice_in_dim(pool_map, first_group, groups_local, 0)
    scales_local = lax.dynamic_slice_in_dim(pool_scale, first_group * group_dim, width_local, 0)
    mapped = jnp.einsum(
        "rgc,gcd->rgd",
        pooled.reshape(row_count, groups_local, group_dim),
        maps_local,
        preferred_element_type=jnp.float32,
    )
    mapped = (mapped.reshape(row_count, width_local) * scales_local).astype(jnp.bfloat16)
    projected = jnp.dot(
        lax.all_gather(mapped, "tp", axis=1, tiled=True),
        out_weight,
        preferred_element_type=jnp.float32,
    )
    return projected.astype(jnp.bfloat16)


def expert_half(expert_input, norm_gain, routes, route_weight, gate_weight, up_weight, down_weight):
    row_count, model_width = expert_input.shape
    top_count = routes.shape[1]
    widened = expert_input.astype(jnp.float32)
    normed = (
        widened
        * lax.rsqrt(jnp.mean(widened * widened, axis=1, keepdims=True) + epsilon)
        * norm_gain
    )
    normed = normed.astype(jnp.bfloat16)
    ep_count = lax.axis_size("ep")
    tp_count = lax.axis_size("tp")
    experts = ep_count * tp_count
    capacity = 2 * row_count * top_count // experts
    copies = row_count * top_count
    flat_routes = routes.reshape(copies)
    onehot = (flat_routes[:, None] == jnp.arange(experts, dtype=jnp.int32)[None, :]).astype(
        jnp.int32
    )
    slot_index = jnp.sum((jnp.cumsum(onehot, axis=0) - onehot) * onehot, axis=1)
    target = flat_routes * capacity + slot_index
    source_row = jnp.arange(copies, dtype=jnp.int32) // top_count
    slot_table = jnp.full((experts * capacity,), row_count, jnp.int32).at[target].set(source_row)
    padded = jnp.concatenate([normed, jnp.zeros((1, model_width), jnp.bfloat16)], axis=0)
    outgoing = padded[slot_table].reshape(experts, capacity, model_width)
    results = expert_rows(
        lax.all_to_all(outgoing, ("ep", "tp"), split_axis=0, concat_axis=0, tiled=True),
        gate_weight,
        up_weight,
        down_weight,
    )
    returned = lax.all_to_all(results, ("ep", "tp"), split_axis=0, concat_axis=0, tiled=True)
    returned = returned.reshape(experts * capacity, model_width)
    picked = returned[target].astype(jnp.float32) * route_weight.reshape(copies)[:, None]
    return picked.reshape(row_count, top_count, model_width).sum(axis=1).astype(jnp.bfloat16)


def on_device(
    pool_input,
    pool_map,
    pool_scale,
    out_weight,
    expert_input,
    norm_gain,
    routes,
    route_weight,
    gate_weight,
    up_weight,
    down_weight,
):
    pool_output = pool_half(pool_input, pool_map, pool_scale, out_weight)
    expert_output = expert_half(
        expert_input, norm_gain, routes, route_weight, gate_weight, up_weight, down_weight
    )
    return (pool_output, expert_output)


def solution(mesh):
    return jax.shard_map(
        on_device,
        mesh=mesh,
        in_specs=(
            P(("grp", "ep"), "tp"),
            P(),
            P(),
            P(None, "tp"),
            P(("grp", "ep", "tp"), None),
            P(),
            P(("grp", "ep", "tp"), None),
            P(("grp", "ep", "tp"), None),
            P(("ep", "tp"), None, None),
            P(("ep", "tp"), None, None),
            P(("ep", "tp"), None, None),
        ),
        out_specs=(P(("grp", "ep"), "tp"), P(("grp", "ep", "tp"), None)),
        check_vma=False,
    )
```

profile of v0, /device:TPU:0, one launch (start us, length us, event | category | flops | bytes accessed | tf_op | source)
XLA Modules:
  0.0 192.7 jit_solution(14643236694304669269)
XLA Ops:
  7.2 0.0 copy-start
  7.2 0.9 copy.19
  8.1 0.1 eq.31
  8.3 0.1 eq.27
  8.4 0.7 broadcast_multiply_fusion
  9.1 0.6 reduce-window.6
  9.7 0.2 slice_reduce_fusion
  9.9 0.1 copy.18
  10.0 0.1 mul.83
  10.2 0.1 fusion.43
  10.3 1.4 scatter_custom_fusion
  11.7 1.2 fusion.11
  12.9 1.2 fusion.13
  14.2 3.3 %gather_fusion = bf16[512,2048]{1,0:T(8,128)(2,1)} fusion(bf16[129,2048]{1,0:T(8,128)(2,1)S(1)} %concatenate.7, s32[1024]{0:T(1024)S(1)} %pad_clamp_fusion.1), kind=kCustom, calls=%fused_computation | custom fusion | bytes 4196352 | tf_op jit(solution)/shard_map/gather | solution.py:86
  17.6 7.5 %all-to-all-start = ((bf16[16,32,2048]{2,1,0:T(8,128)(2,1)}), bf16[16,32,2048]{2,1,0:T(8,128)(2,1)}, u32[]{:S(2)}, u32[]{:S(2)}) async-start(bf16[16,32,2048]{2,1,0:T(8,128)(2,1)} %bitcast.57), calls=%async_computation | async-start | bytes 4194304 | tf_op jit(solution)/shard_map/all_to_all | solution.py:88
  25.0 0.7 slice.58
  25.8 2.2 %collective-permute-start = (bf16[16,256]{1,0:T(8,128)(2,1)S(1)}, bf16[16,256]{1,0:T(8,128)(2,1)S(1)}, u32[]{:S(2)}, u32[]{:S(2)}) collective-permute-start(bf16[16,256]{1,0:T(8,128)(2,1)S(1)} %slice.58), channel_id=1, source_target_pairs={{0,4},{4,8},{8,12},{1,5},{5,9},{9,13},{2,6},{6,10},{10,14},{3,7},{... | collective-permute-start | bytes 24584 | tf_op jit(solution)/shard_map/ppermute | solution.py:13
  28.2 0.8 dynamic_slice.7
  29.0 0.0 collective-permute-done
  29.0 1.1 maximum_convert_fusion
  30.1 44.3 %all-to-all-done = bf16[16,32,2048]{2,1,0:T(8,128)(2,1)} async-done(((bf16[16,32,2048]{2,1,0:T(8,128)(2,1)}), bf16[16,32,2048]{2,1,0:T(8,128)(2,1)}, u32[]{:S(2)}, u32[]{:S(2)}) %all-to-all-start) | async-done | bytes 2097184 | tf_op jit(solution)/shard_map/all_to_all | solution.py:88
  74.4 4.4 %fusion.3 = f32[512,512]{1,0:T(8,128)} fusion(bf16[512,2048]{1,0:T(8,128)(2,1)} %bitcast.6, bf16[1,2048,512]{2,1,0:T(8,128)(2,1)} %param.19), kind=kOutput, calls=%fused_computation.7 | convolution fusion | flops 1073741824 | bytes 5242880 | tf_op jit(solution)/shard_map/dot_general | solution.py:19
  78.9 0.0 copy-done
  78.9 6.3 %convolution_convert_fusion = bf16[512,2048]{1,0:T(8,128)(2,1)} fusion(bf16[1,512,2048]{2,1,0:T(8,128)(2,1)S(1)} %copy-done, bf16[512,2048]{1,0:T(8,128)(2,1)} %bitcast.6, bf16[1,2048,512]{2,1,0:T(8,128)(2,1)} %param.20, f32[512,512]{1,0:T(8,128)} %fusion.3), kind=kOutput, calls=%fused_computation.3 | convolution fusion | flops 2150105088 | bytes 9437184 | tf_op jit(solution)/shard_map/dot_general | solution.py:22
  85.1 4.4 %all-to-all-start.1 = ((bf16[16,32,2048]{2,1,0:T(8,128)(2,1)}), bf16[16,32,2048]{2,1,0:T(8,128)(2,1)}, u32[]{:S(2)}, u32[]{:S(2)}) async-start(bf16[16,32,2048]{2,1,0:T(8,128)(2,1)} %bitcast.58), calls=%async_computation.1 | async-start | bytes 4194304 | tf_op jit(solution)/shard_map/all_to_all | solution.py:93
  89.6 0.2 all-gather.2.cloned.1.call-start
  89.8 3.8 %fusion.35 = f32[2,128,1024]{2,1,0:T(8,128)S(1)} fusion(bf16[8,128,128]{2,1,0:T(8,128)(2,1)} %param.12, s32[]{:T(128)S(6)} %select_n.92, s32[256]{0:T(256)S(1)} %fusion.46, s32[1024]{0:T(1024)S(1)} %add_add_fusion, f32[1040,256]{1,0:T(8,128)S(1)} %maximum_convert_fusion, pred[256]{0:T(512)(128)(4,1)S(1)} %get-tuple-element.2, ...), kind=kOutput, calls=%fused_computation.54 | convolution fusion | flops 76546048 | bytes 17904644 | tf_op jit(solution)/shard_map/rgc,gcd->rgd/dot_general | solution.py:47
  93.7 0.0 copy-start.1
  93.7 0.0 copy-start.2
  93.7 0.9 fusion.31
  94.6 0.0 all-gather.2.cloned.1.call-update
  94.6 0.0 copy-done.1
  94.6 0.1 copy.22
  94.8 75.0 %all-gather.2.cloned.1.call-done = bf16[1024,1024]{0,1:T(8,128)(2,1)} async-done(((bf16[1024,256]{0,1:T(8,128)(2,1)}), bf16[1024,1024]{0,1:T(8,128)(2,1)}) %all-gather.2.cloned.1.call-update) | async-done | bytes 2097168 | tf_op jit(solution)/shard_map/all_gather | solution.py:55
  169.8 0.0 copy-done.2
  169.8 3.9 %convolution_convert_fusion.1 = bf16[1024,512]{1,0:T(8,128)(2,1)} fusion(bf16[1024,1024]{0,1:T(8,128)(2,1)} %all-gather.2.cloned.1.call-done, bf16[1024,512]{1,0:T(8,128)(2,1)S(1)} %copy-done.2), kind=kOutput, calls=%fused_computation.10 | convolution fusion | flops 1074266112 | bytes 4194304 | tf_op jit(solution)/shard_map/dot_general | solution.py:54
  173.6 0.0 all-to-all-done.1
  173.6 4.2 %gather_fusion.1 = bf16[256,2048]{1,0:T(8,128)(2,1)S(1)} fusion(bf16[512,2048]{1,0:T(8,128)(2,1)} %bitcast.11, s32[1024]{0:T(1024)S(1)} %pad_clamp_fusion), kind=kCustom, calls=%fused_computation.1 | custom fusion | bytes 2098176 | tf_op jit(solution)/shard_map/gather | solution.py:95
  177.9 2.4 %reshape.127 = f32[128,2,2048]{2,1,0:T(2,128)} reshape(bf16[256,2048]{1,0:T(8,128)(2,1)S(1)} %gather_fusion.1) | data formatting | bytes 3145728 | tf_op jit(solution)/shard_map/convert_element_type | solution.py:95
  180.2 5.6 %multiply_reduce_fusion = bf16[128,2048]{1,0:T(8,128)(2,1)} fusion(f32[128,2,2048]{2,1,0:T(2,128)} %reshape.127, f32[128,2]{1,0:T(8,128)S(1)} %copy.22), kind=kLoop, calls=%fused_computation.9 | loop fusion | flops 786432 | bytes 2622464 | tf_op jit(solution)/shard_map/reduce_sum | solution.py:96
  (20 shorter events, 0.3 us)
Async XLA Ops:
  7.2 71.7 %copy-start = (bf16[1,512,2048]{2,1,0:T(8,128)(2,1)S(1)}, bf16[1,512,2048]{2,1,0:T(8,128)(2,1)}, u32[]{:S(2)}) copy-start(bf16[1,512,2048]{2,1,0:T(8,128)(2,1)} %param.21) | copy-start | bytes 6291460
  17.6 56.8 %all-to-all-start = ((bf16[16,32,2048]{2,1,0:T(8,128)(2,1)}), bf16[16,32,2048]{2,1,0:T(8,128)(2,1)}, u32[]{:S(2)}, u32[]{:S(2)}) async-start(bf16[16,32,2048]{2,1,0:T(8,128)(2,1)} %bitcast.57), calls=%async_computation | async-start | bytes 4194304 | tf_op jit(solution)/shard_map/all_to_all | solution.py:88
  25.8 3.2 %collective-permute-start = (bf16[16,256]{1,0:T(8,128)(2,1)S(1)}, bf16[16,256]{1,0:T(8,128)(2,1)S(1)}, u32[]{:S(2)}, u32[]{:S(2)}) collective-permute-start(bf16[16,256]{1,0:T(8,128)(2,1)S(1)} %slice.58), channel_id=1, source_target_pairs={{0,4},{4,8},{8,12},{1,5},{5,9},{9,13},{2,6},{6,10},{10,14},{3,7},{... | collective-permute-start | bytes 24584 | tf_op jit(solution)/shard_map/ppermute | solution.py:13
  85.1 88.5 %all-to-all-start.1 = ((bf16[16,32,2048]{2,1,0:T(8,128)(2,1)}), bf16[16,32,2048]{2,1,0:T(8,128)(2,1)}, u32[]{:S(2)}, u32[]{:S(2)}) async-start(bf16[16,32,2048]{2,1,0:T(8,128)(2,1)} %bitcast.58), calls=%async_computation.1 | async-start | bytes 4194304 | tf_op jit(solution)/shard_map/all_to_all | solution.py:93
  89.6 80.2 %all-gather.2.cloned.1.call-start = ((), (), s32[]{:S(2)}) async-start(), calls=%async_computation.2 | async-start | bytes 2621440 | tf_op jit(solution)/shard_map/all_gather | solution.py:55
  93.7 1.0 copy-start.1
  93.7 76.1 %copy-start.2 = (bf16[1024,512]{1,0:T(8,128)(2,1)S(1)}, bf16[1024,512]{1,0:T(8,128)(2,1)}, u32[]{:S(2)}) copy-start(bf16[1024,512]{1,0:T(8,128)(2,1)} %param.14) | copy-start | bytes 3145732
Sparse Core Ops, SparseCore 0:
  94.7 74.9 all-gather.1
where the time goes:
time: 193 us
  waiting for transfers between devices  119 us (62%)
  matrix products  18.4 us (10%)
  local copies, waits for them, and re-layouts  14.6 us (8%)
  starting transfers between devices  14.4 us (7%)
  between operations  14.2 us (7%)
  other arithmetic  11.7 us (6%)
    all_gather x1, waiting for transfers between devices, pool_half(): lax.all_gather(mapped, 'tp', axis=1, tiled=True)  75 us
    all_to_all x1, waiting for transfers between devices, expert_half(): lax.all_to_all(outgoing, ('ep', 'tp'), split_axis=0, concat_axis=0, tiled...  44.3 us
    all_to_all x1, starting transfers between devices, expert_half(): lax.all_to_all(outgoing, ('ep', 'tp'), split_axis=0, concat_axis=0, tiled...  7.46 us
    dot_general x1, matrix products, expert_rows(): jnp.dot(hidden, down_weight[0], preferred_element_type=jnp.float32)  6.28 us
    reduce_sum x1, other arithmetic, expert_half(): picked.reshape(row_count, top_count, model_width).sum(axis=1)  5.59 us
    dot_general x1, matrix products, expert_rows(): jnp.dot(flat_rows, gate_weight[0], preferred_element_type=jnp.float32)  4.44 us
    all_to_all x1, starting transfers between devices, expert_half(): lax.all_to_all(results, ('ep', 'tp'), split_axis=0, concat_axis=0, tiled=...  4.44 us
    gather x1, local copies, waits for them, and re-layouts, expert_half(): returned[target].astype(jnp.float32) * route_weight.reshape(copies)[:, None]  4.22 us
  transfers between devices with their start and end apart: 4, of which 2 were waited for; matrix products, arithmetic and copies ran while one was open for 6% of the time, Pallas kernels for 0%

commit v1 on v0

v1 whole, which is shorter than its diff:
```python
import functools

import jax
import jax.numpy as jnp
from jax import lax
from jax.experimental import pallas as pl
from jax.experimental.pallas import tpu as pltpu
from jax.sharding import PartitionSpec as P

epsilon = 1e-06
halo_depth = 16
MESH = pl.DeviceIdType.MESH
bf16 = jnp.bfloat16
f32 = jnp.float32


def shifted_2(shard, axis, by):
    size = lax.axis_size(axis)
    pairs = [(i, i + by) for i in range(size) if 0 <= i + by < size]
    return lax.ppermute(shard, axis, pairs)


def mapped_channels(pool_input, pool_map, pool_scale):
    row_count, width_local = pool_input.shape
    group_dim = pool_map.shape[1]
    groups_local = width_local // group_dim
    last_rows = pool_input[row_count - halo_depth :]
    earlier_rows = shifted_2(last_rows, "ep", 1)
    extended = jnp.concatenate([earlier_rows, pool_input], axis=0).astype(f32)
    first_group = lax.axis_index("tp") * groups_local
    group_ids = first_group + jnp.arange(width_local, dtype=jnp.int32) // group_dim
    window = jnp.left_shift(jnp.int32(2), group_ids % 4)
    summed = jnp.zeros((row_count, width_local), f32)
    for offset in range(halo_depth):
        shifted = extended[halo_depth - offset : halo_depth - offset + row_count]
        summed = summed + jnp.where(offset < window, shifted, 0.0)
    positions = lax.axis_index("ep") * row_count + jnp.arange(row_count, dtype=jnp.int32)
    counted = jnp.minimum(positions[:, None] + 1, window[None, :]).astype(f32)
    pooled = (summed / counted - extended[halo_depth:]).astype(bf16)
    maps_local = lax.dynamic_slice_in_dim(pool_map, first_group, groups_local, 0)
    scales_local = lax.dynamic_slice_in_dim(pool_scale, first_group * group_dim, width_local, 0)
    mapped = jnp.einsum(
        "rgc,gcd->rgd",
        pooled.reshape(row_count, groups_local, group_dim),
        maps_local,
        preferred_element_type=f32,
    )
    return (mapped.reshape(row_count, width_local) * scales_local).astype(bf16)


def route_codes(routes, route_weight, n_ep, n_tp, capacity):
    row_count, top = routes.shape
    experts = n_ep * n_tp
    flat = routes.reshape(row_count * top)
    onehot = (flat[:, None] == jnp.arange(experts, dtype=jnp.int32)[None, :]).astype(f32)
    copies = row_count * top
    earlier = (
        jnp.arange(copies, dtype=jnp.int32)[:, None] > jnp.arange(copies, dtype=jnp.int32)[None, :]
    ).astype(f32)
    before = jnp.dot(earlier, onehot, preferred_element_type=f32)
    slot = jnp.sum(before * onehot, axis=1).astype(jnp.int32)
    code = (flat % n_tp) * (n_ep * capacity) + (flat // n_tp) * capacity + slot
    codes = code.reshape(row_count, top).T.astype(f32)
    meta = jnp.concatenate([codes, route_weight.T.astype(f32)], axis=0)
    return jnp.pad(meta, ((0, -meta.shape[0] % 8), (0, 0)))


def kernel(
    n, n_ep, cap, top,
    x_ref, meta_ref, pool_ref, gate_hbm, up_hbm, down_hbm, out_w_hbm,
    pool_out, expert_out,
    wg, wu, wd, wo, tok, meta, pools, packed, rows, back, hidden, part, from_left, from_right, acc,
    w_sem, tok_recv, tok_right, tok_left, meta_recv, meta_right, meta_left,
    pool_recv, pool_right, pool_left, pk_send, pk_recv, bk_send, bk_recv,
    rs_right, rs_right_recv, rs_left, rs_left_recv,
):
    me = lax.axis_index("tp")
    mine = lax.axis_index("ep")
    slots = n_ep * cap
    width = x_ref.shape[1]
    d_expert = wg.shape[1]
    shard = pool_ref.shape[1]
    has_left, has_right = me > 0, me < n - 1

    def peer(q):
        return lax.rem(mine + q, n_ep)

    def at_slots(p):
        return pl.ds(pl.multiple_of(p * cap, cap), cap)

    loads = [
        pltpu.make_async_copy(src, dst, w_sem.at[i])
        for i, (src, dst) in enumerate(
            ((gate_hbm.at[0], wg), (up_hbm.at[0], wu), (down_hbm.at[0], wd), (out_w_hbm, wo))
        )
    ]
    for load in loads:
        load.start()

    barrier = pltpu.get_barrier_semaphore()

    @pl.when(has_left)
    def _():
        pl.semaphore_signal(barrier, inc=1, device_id={"tp": me - 1}, device_id_type=MESH)

    @pl.when(has_right)
    def _():
        pl.semaphore_signal(barrier, inc=1, device_id={"tp": me + 1}, device_id_type=MESH)

    for q in range(1, n_ep):
        pl.semaphore_signal(barrier, inc=1, device_id={"ep": peer(q)}, device_id_type=MESH)
    neighbours = jnp.where(has_left, 1, 0) + jnp.where(has_right, 1, 0)
    pl.semaphore_wait(barrier, n_ep - 1 + neighbours)

    def source(j):
        least = jnp.minimum(me, n - 1 - me)
        k = (j + 1) // 2
        near = jnp.where(j % 2 == 1, me - k, me + k)
        k_far = j - least
        far = jnp.where(me > n - 1 - me, me - k_far, me + k_far)
        return jnp.where(j <= 2 * least, near, far)

    def hop(src, buffer, s, send, recv, step):
        return pltpu.make_async_remote_copy(
            src_ref=src, dst_ref=buffer.at[s], send_sem=send.at[s], recv_sem=recv.at[s],
            device_id={"tp": me + step}, device_id_type=MESH,
        )

    token_lane = ((tok, tok_right, tok_left, tok_recv), (meta, meta_right, meta_left, meta_recv))
    pool_lane = ((pools, pool_right, pool_left, pool_recv),)

    def pass_on(lane, s, own):
        @pl.when((s <= me) & has_right)
        def _():
            for i, (buffer, right, left, recv) in enumerate(lane):
                hop(own[i] if own else buffer.at[s], buffer, s, right, recv, 1).start()

        @pl.when((s >= me) & has_left)
        def _():
            for i, (buffer, right, left, recv) in enumerate(lane):
                hop(own[i] if own else buffer.at[s], buffer, s, left, recv, -1).start()

    def arrive(lane, s):
        for buffer, right, left, recv in lane:
            hop(buffer.at[s], buffer, s, right, recv, 1).wait_recv()

    def passed(lane, s, own):
        @pl.when((s <= me) & has_right)
        def _():
            for buffer, right, left, recv in lane:
                hop(buffer.at[s], buffer, s, right, recv, 1).wait_send()

        @pl.when((s >= me) & has_left)
        def _():
            for buffer, right, left, recv in lane:
                hop(buffer.at[s], buffer, s, left, recv, -1).wait_send()

    def exchange(src, dst, s, p, send, recv):
        return pltpu.make_async_remote_copy(
            src_ref=src.at[s, at_slots(p)], dst_ref=dst.at[s, at_slots(mine)],
            send_sem=send.at[s, p], recv_sem=recv.at[s, mine],
            device_id={"ep": p}, device_id_type=MESH,
        )

    def exchanged(dst, s, p, send, recv):
        return pltpu.make_async_remote_copy(
            src_ref=dst.at[s, at_slots(p)], dst_ref=dst.at[s, at_slots(p)],
            send_sem=send.at[s, p], recv_sem=recv.at[s, p],
            device_id={"ep": p}, device_id_type=MESH,
        )

    def tiles(total, size):
        return total // size, lambda i: pl.ds(pl.multiple_of(i * size, size), size)

    def slot_masks(s, use_weight):
        row = lax.broadcasted_iota(jnp.int32, (slots, x_ref.shape[0]), 0) + me * slots
        row = row.astype(f32)
        held = meta[s]
        total = jnp.zeros((slots, x_ref.shape[0]), f32)
        for k in range(top):
            value = held[top + k : top + k + 1] if use_weight else 1.0
            total = total + jnp.where(row == held[k : k + 1], value, 0.0)
        return total

    tile_w = min(512, width)
    count_w, at_w = tiles(width, tile_w)
    tile_h = min(256, d_expert)
    count_h, at_h = tiles(d_expert, tile_h)
    tile_r = min(256, pool_ref.shape[0])
    count_r, at_r = tiles(pool_ref.shape[0], tile_r)

    def pack(s):
        choose = slot_masks(s, False).astype(bf16)

        def tile(i, _):
            packed[s, :, at_w(i)] = jnp.dot(
                choose, tok[s, :, at_w(i)], preferred_element_type=f32
            ).astype(bf16)
            return 0

        lax.fori_loop(0, count_w, tile, 0)
        for q in range(1, n_ep):
            exchange(packed, rows, s, peer(q), pk_send, pk_recv).start()
        rows[s, at_slots(mine)] = packed[s, at_slots(mine)]

    def expert(s):
        for q in range(1, n_ep):
            exchanged(rows, s, peer(q), pk_send, pk_recv).wait_recv()

        def inner(i, _):
            here = rows[s]
            gate = jnp.dot(here, wg[:, at_h(i)], preferred_element_type=f32)
            up = jnp.dot(here, wu[:, at_h(i)], preferred_element_type=f32)
            hidden[:, at_h(i)] = (gate / (1.0 + jnp.exp(-gate)) * up).astype(bf16)
            return 0

        lax.fori_loop(0, count_h, inner, 0)

        def outer(i, _):
            rows[s, :, at_w(i)] = jnp.dot(
                hidden[...], wd[:, at_w(i)], preferred_element_type=f32
            ).astype(bf16)
            return 0

        lax.fori_loop(0, count_w, outer, 0)
        for q in range(1, n_ep):
            exchange(rows, back, s, peer(q), bk_send, bk_recv).start()
        back[s, at_slots(mine)] = rows[s, at_slots(mine)]

    def rs_hop(src, buffer, d, send, recv, step):
        return pltpu.make_async_remote_copy(
            src_ref=src.at[d], dst_ref=buffer.at[d], send_sem=send.at[d], recv_sem=recv.at[d],
            device_id={"tp": me + step}, device_id_type=MESH,
        )

    def combine(s):
        for q in range(1, n_ep):
            exchanged(back, s, peer(q), bk_send, bk_recv).wait_recv()
        weights = slot_masks(s, True)
        high = weights.astype(bf16)
        low = (weights - high.astype(f32)).astype(bf16)
        dims = (((0,), (0,)), ((), ()))

        def tile(i, _):
            here = back[s, :, at_w(i)]
            part[s, :, at_w(i)] = (
                lax.dot_general(high, here, dims, preferred_element_type=f32)
                + lax.dot_general(low, here, dims, preferred_element_type=f32)
            ).astype(bf16)
            return 0

        lax.fori_loop(0, count_w, tile, 0)

        @pl.when((me == 0) & (s > me))
        def _():
            rs_hop(part, from_left, s, rs_right, rs_right_recv, 1).start()

        @pl.when((me == n - 1) & (s < me))
        def _():
            rs_hop(part, from_right, s, rs_left, rs_left_recv, -1).start()

    def project(s, first):
        def tile(i, _):
            lhs = pool_ref[at_r(i), :] if first else pools[s, at_r(i), :]
            product = jnp.dot(
                lhs, wo[pl.ds(pl.multiple_of(s * shard, shard), shard), :],
                preferred_element_type=f32,
            )
            acc[at_r(i), :] = product if first else acc[at_r(i), :] + product
            return 0

        lax.fori_loop(0, count_r, tile, 0)

    def add_into(buffer, d):
        def tile(i, _):
            buffer[d, :, at_w(i)] = (
                buffer[d, :, at_w(i)].astype(f32) + part[d, :, at_w(i)].astype(f32)
            ).astype(bf16)
            return 0

        lax.fori_loop(0, count_w, tile, 0)

    pass_on(token_lane, me, (x_ref, meta_ref))

    def own(i, _):
        tok[me, :, at_w(i)] = x_ref[:, at_w(i)]
        return 0

    lax.fori_loop(0, count_w, own, 0)
    meta[me] = meta_ref[...]
    loads[3].wait()
    project(me, True)

    def step(j, _):
        @pl.when(j < n)
        def _():
            s = source(j)

            @pl.when(j > 0)
            def _():
                arrive(token_lane, s)
                pass_on(token_lane, s, None)

            @pl.when((s == 0) & has_right)
            def _():
                hop(pool_ref, pools, me, pool_right, pool_recv, 1).start()

            @pl.when((s == n - 1) & has_left)
            def _():
                hop(pool_ref, pools, me, pool_left, pool_recv, -1).start()

            pack(s)

        @pl.when(j == 1)
        def _():
            for load in loads[:3]:
                load.wait()

        @pl.when((j >= 1) & (j <= n))
        def _():
            expert(source(j - 1))

        @pl.when(j >= 2)
        def _():
            combine(source(j - 2))

        return 0

    lax.fori_loop(0, n + 2, step, 0)

    def tail(i, _):
        s = source(i + 1)
        arrive(pool_lane, s)
        pass_on(pool_lane, s, None)
        project(s, False)
        right, left = i + 1, n - 2 - i

        @pl.when((me > 0) & (me < right))
        def _():
            rs_hop(part, from_left, right, rs_right, rs_right_recv, 1).wait_recv()
            add_into(from_left, right)
            rs_hop(from_left, from_left, right, rs_right, rs_right_recv, 1).start()

        @pl.when((me < n - 1) & (me > left))
        def _():
            rs_hop(part, from_right, left, rs_left, rs_left_recv, -1).wait_recv()
            add_into(from_right, left)
            rs_hop(from_right, from_right, left, rs_left, rs_left_recv, -1).start()

        return 0

    lax.fori_loop(0, n - 1, tail, 0)
    pool_out[...] = acc[...].astype(bf16)
    expert_total = part[me].astype(f32)
    acc_rows = expert_out

    @pl.when(has_left)
    def _():
        rs_hop(part, from_left, me, rs_right, rs_right_recv, 1).wait_recv()

    @pl.when(has_right)
    def _():
        rs_hop(part, from_right, me, rs_left, rs_left_recv, -1).wait_recv()

    @pl.when(has_left & has_right)
    def _():
        acc_rows[...] = (
            expert_total + from_left[me].astype(f32) + from_right[me].astype(f32)
        ).astype(bf16)

    @pl.when(has_left & jnp.logical_not(has_right))
    def _():
        acc_rows[...] = (expert_total + from_left[me].astype(f32)).astype(bf16)

    @pl.when(has_right & jnp.logical_not(has_left))
    def _():
        acc_rows[...] = (expert_total + from_right[me].astype(f32)).astype(bf16)

    def drain(s, _):
        passed(token_lane, s, None)
        passed(pool_lane, s, None)
        for q in range(1, n_ep):
            exchange(packed, rows, s, peer(q), pk_send, pk_recv).wait_send()
            exchange(rows, back, s, peer(q), bk_send, bk_recv).wait_send()

        @pl.when(me < s)
        def _():
            rs_hop(part, from_left, s, rs_right, rs_right_recv, 1).wait_send()

        @pl.when(me > s)
        def _():
            rs_hop(part, from_right, s, rs_left, rs_left_recv, -1).wait_send()

        return 0

    lax.fori_loop(0, n, drain, 0)


def on_device(
    pool_input, pool_map, pool_scale, out_weight, expert_input, norm_gain,
    routes, route_weight, gate_weight, up_weight, down_weight,
):
    n_ep, n = lax.axis_size("ep"), lax.axis_size("tp")
    tokens, width = expert_input.shape
    top = routes.shape[1]
    cap = max(2 * tokens * top // (n_ep * n), 16)
    slots = n_ep * cap
    widened = expert_input.astype(f32)
    normed = widened * lax.rsqrt(jnp.mean(widened * widened, axis=1, keepdims=True) + epsilon)
    normed = (normed * norm_gain).astype(bf16)
    meta = route_codes(routes, route_weight, n_ep, n, cap)
    mapped = mapped_channels(pool_input, pool_map, pool_scale)
    d_expert = gate_weight.shape[2]
    dma = pltpu.SemaphoreType.DMA
    vmem = pl.BlockSpec(memory_space=pltpu.VMEM)
    hbm = pl.BlockSpec(memory_space=pl.ANY)
    line = dma((n,))
    pair = dma((n, n_ep))
    return pl.pallas_call(
        functools.partial(kernel, n, n_ep, cap, top),
        out_shape=(
            jax.ShapeDtypeStruct((mapped.shape[0], out_weight.shape[1]), bf16),
            jax.ShapeDtypeStruct((tokens, width), bf16),
        ),
        in_specs=[vmem] * 3 + [hbm] * 4,
        out_specs=(vmem, vmem),
        scratch_shapes=[
            pltpu.VMEM((width, d_expert), bf16),
            pltpu.VMEM((width, d_expert), bf16),
            pltpu.VMEM((d_expert, width), bf16),
            pltpu.VMEM(out_weight.shape, bf16),
            pltpu.VMEM((n, tokens, width), bf16),
            pltpu.VMEM((n,) + meta.shape, f32),
            pltpu.VMEM((n,) + mapped.shape, bf16),
            pltpu.VMEM((n, slots, width), bf16),
            pltpu.VMEM((n, slots, width), bf16),
            pltpu.VMEM((n, slots, width), bf16),
            pltpu.VMEM((slots, d_expert), bf16),
            pltpu.VMEM((n, tokens, width), bf16),
            pltpu.VMEM((n, tokens, width), bf16),
            pltpu.VMEM((n, tokens, width), bf16),
            pltpu.VMEM((mapped.shape[0], out_weight.shape[1]), f32),
            dma((4,)),
            line, line, line, line, line, line, line, line, line,
            pair, pair, pair, pair,
            line, line, line, line,
        ],
        compiler_params=pltpu.CompilerParams(
            collective_id=0, has_side_effects=True, vmem_limit_bytes=62 * 1024 * 1024
        ),
    )(normed, meta, mapped, gate_weight, up_weight, down_weight, out_weight)


def solution(mesh):
    return jax.shard_map(
        on_device,
        mesh=mesh,
        in_specs=(
            P(("grp", "ep"), "tp"),
            P(),
            P(),
            P(None, "tp"),
            P(("grp", "ep", "tp"), None),
            P(),
            P(("grp", "ep", "tp"), None),
            P(("grp", "ep", "tp"), None),
            P(("ep", "tp"), None, None),
            P(("ep", "tp"), None, None),
            P(("ep", "tp"), None, None),
        ),
        out_specs=(P(("grp", "ep"), "tp"), P(("grp", "ep", "tp"), None)),
        check_vma=False,
    )
```

time: 193 us -> 142 us (0.74)
  Pallas kernels: 0 us -> 123 us
  waiting for transfers between devices: 119 us -> 0.01 us
  matrix products: 18.4 us -> 3.22 us
  between operations: 14.2 us -> 0.79 us
  starting transfers between devices: 14.4 us -> 2.38 us
  local copies, waits for them, and re-layouts: 14.6 us -> 6.16 us
  other arithmetic: 11.7 us -> 5.33 us
    pallas_call x0 -> x1, Pallas kernels: none -> 123 us  [on_device(): pl.pallas_call(functools.partial(kernel, n, n_ep, cap, top), out_shape=(j...]
    all_gather x1 -> x0, waiting for transfers between devices: 75 us -> none  [pool_half(): lax.all_gather(mapped, 'tp', axis=1, tiled=True)]
    all_to_all x2 -> x0, waiting for transfers between devices: 44.3 us -> none  [the longest x1 44.3 us: expert_half(): lax.all_to_all(outgoing, ('ep', 'tp'), split_axis=0, concat_axis=0, tiled...]
    dot_general x4 -> x2, matrix products: 18.4 us -> 3.22 us  [the longest x1 3.01 us: mapped_channels(): jnp.einsum('rgc,gcd->rgd', pooled.reshape(row_count, groups_local, group_...]
    all_to_all x2 -> x0, starting transfers between devices: 11.9 us -> none  [the longest x1 7.46 us: expert_half(): lax.all_to_all(outgoing, ('ep', 'tp'), split_axis=0, concat_axis=0, tiled...]
    gather x2 -> x0, local copies, waits for them, and re-layouts: 7.57 us -> none  [the longest x1 4.22 us: expert_half(): returned[target].astype(jnp.float32) * route_weight.reshape(copies)[:, None]]
    reduce_sum x3 -> x1, other arithmetic: 6.9 us -> 1.23 us  [on_device(): jnp.mean(widened * widened, axis=1, keepdims=True) + epsilon]
    unnamed x8 -> x13, local copies, waits for them, and re-layouts: 1.07 us -> 3.93 us
  transfers between devices with their start and end apart: 4 -> 1, of which waited for: 2 -> 0; matrix products, arithmetic and copies ran while one was open for 6% -> 5% of each run, Pallas kernels for 0% -> 0%
where the time goes in v1:
time: 142 us; the launch traced here: 141 us
  Pallas kernels  123 us (87%)
  local copies, waits for them, and re-layouts  6.16 us (4%)
  other arithmetic  5.33 us (4%)
  matrix products  3.22 us (2%)
  starting transfers between devices  2.38 us (2%)
    pallas_call x1, Pallas kernels, on_device(): pl.pallas_call(functools.partial(kernel, n, n_ep, cap, top), out_shape=(j...  123 us
    unnamed x13, local copies, waits for them, and re-layouts  3.93 us
    dot_general x1, matrix products, mapped_channels(): jnp.einsum('rgc,gcd->rgd', pooled.reshape(row_count, groups_local, group_...  3.01 us
  transfers between devices with their start and end apart: 1, of which 0 were waited for; matrix products, arithmetic and copies ran while one was open for 5% of the time, Pallas kernels for 0%

profile of v1, /device:TPU:0, one launch (start us, length us, event | category | flops | bytes accessed | tf_op | source)
XLA Modules:
  0.0 140.6 jit_solution(7600924894811609280)
XLA Ops:
  0.6 0.0 copy-start
  0.6 0.0 copy-start.1
  0.7 0.0 copy-start.2
  0.7 0.0 copy-start.4
  0.7 0.8 slice.52
  1.5 2.4 %collective-permute-start = (bf16[16,256]{1,0:T(8,128)(2,1)S(1)}, bf16[16,256]{1,0:T(8,128)(2,1)S(1)}, u32[]{:S(2)}, u32[]{:S(2)}) collective-permute-start(bf16[16,256]{1,0:T(8,128)(2,1)S(1)} %slice.52), channel_id=1, source_target_pairs={{0,4},{4,8},{8,12},{1,5},{5,9},{9,13},{2,6},{6,10},{10,14},{3,7},{... | collective-permute-start | bytes 24584 | tf_op jit(solution)/shard_map/ppermute | solution.py:20
  4.0 1.2 fusion.1
  5.3 0.8 copy.16
  6.1 0.1 eq.18
  6.2 0.2 fusion
  6.4 0.1 convert_element_type.38
  6.6 0.1 copy.17
  6.6 0.7 convert_bitcast_fusion
  7.4 0.0 copy-done.1
  7.4 1.7 %fusion.3.x_ref = bf16[128,2048]{1,0:T(8,128)(2,1)} fusion(bf16[128,2048]{1,0:T(8,128)(2,1)S(1)} %copy-done.1, f32[2048]{0:T(1024)} %param.16, f32[128]{0:T(128)S(1)} %add_rsqrt_fusion), kind=kLoop, calls=%fused_computation.6 | loop fusion | flops 1048576 | bytes 1057280 | tf_op jit(solution)/shard_map/convert_element_type | solution.py:410
  9.0 0.0 copy-done.4
  9.0 0.6 select_maximum_fusion.meta_ref
  9.7 0.8 dynamic_slice.7
  10.4 0.0 collective-permute-done
  10.4 0.0 copy-done.2
  10.4 0.1 maximum_convert_fusion
  10.5 0.0 copy-done
  10.5 3.0 %fusion.22 = f32[2,128,1024]{2,1,0:T(8,128)S(1)} fusion(bf16[8,128,128]{2,1,0:T(8,128)(2,1)S(1)} %copy-done, s32[]{:T(128)S(6)} %select_n.86, s32[256]{0:T(256)S(1)} %fusion.31, s32[1024]{0:T(1024)S(1)} %add_add_fusion, f32[1040,256]{1,0:T(8,128)S(1)} %maximum_convert_fusion, pred[256]{0:T(512)(128)(4,1)S(1)} %get-tuple-element.2, ...), kind=kOutput, calls=%fused_computation.42 | convolution fusion | flops 76546048 | bytes 17904644 | tf_op jit(solution)/shard_map/rgc,gcd->rgd/dot_general | solution.py:42
  13.5 0.3 copy.21
  13.9 0.9 multiply_convert_fusion.pool_ref
  14.8 122.8 %shard_map.122 = (bf16[1024,512]{1,0:T(8,128)(2,1)}, bf16[128,2048]{1,0:T(8,128)(2,1)}) custom-call(bf16[128,2048]{1,0:T(8,128)(2,1)} %fusion.3.x_ref, f32[8,128]{1,0:T(8,128)} %select_maximum_fusion.meta_ref, bf16[1024,256]{1,0:T(8,128)(2,1)} %multiply_convert_fusion.pool_ref, bf16[1,2048,512]{2,1,0:T(8,128)(2,1)} %gate_hbm.1, ...), custom_call_target="tpu_custom_call" | custom-call | tf_op jit(solution)/shard_map/pallas_call | solution.py:419
  137.5 0.0 copy-start.3
  137.5 2.3 %copy.30 = bf16[1024,512]{1,0:T(8,128)(2,1)} copy(bf16[1024,512]{1,0:T(8,128)(2,1)} %get-tuple-element.20) | data formatting | bytes 2097152
  139.8 0.0 copy-done.3
  139.9 0.8 copy.31
  (12 shorter events, 0.2 us)
Async XLA Ops:
  0.6 9.9 %copy-start = (bf16[8,128,128]{2,1,0:T(8,128)(2,1)S(1)}, bf16[8,128,128]{2,1,0:T(8,128)(2,1)}, u32[]{:S(2)}) copy-start(bf16[8,128,128]{2,1,0:T(8,128)(2,1)} %param.12) | copy-start | bytes 786436
  0.6 6.7 %copy-start.1 = (bf16[128,2048]{1,0:T(8,128)(2,1)S(1)}, bf16[128,2048]{1,0:T(8,128)(2,1)}, u32[]{:S(2)}) copy-start(bf16[128,2048]{1,0:T(8,128)(2,1)} %param.15) | copy-start | bytes 1572868
  0.7 9.8 %copy-start.2 = (bf16[1024,256]{1,0:T(8,128)(2,1)S(1)}, bf16[1024,256]{1,0:T(8,128)(2,1)}, u32[]{:S(2)}) copy-start(bf16[1024,256]{1,0:T(8,128)(2,1)} %param.11) | copy-start | bytes 1572868
  0.7 8.4 %copy-start.4 = (f32[128,2]{0,1:T(2,128)S(1)}, f32[128,2]{0,1:T(2,128)}, u32[]{:S(2)}) copy-start(f32[128,2]{0,1:T(2,128)} %param.18) | copy-start | bytes 3076
  1.5 8.9 %collective-permute-start = (bf16[16,256]{1,0:T(8,128)(2,1)S(1)}, bf16[16,256]{1,0:T(8,128)(2,1)S(1)}, u32[]{:S(2)}, u32[]{:S(2)}) collective-permute-start(bf16[16,256]{1,0:T(8,128)(2,1)S(1)} %slice.52), channel_id=1, source_target_pairs={{0,4},{4,8},{8,12},{1,5},{5,9},{9,13},{2,6},{6,10},{10,14},{3,7},{... | collective-permute-start | bytes 24584 | tf_op jit(solution)/shard_map/ppermute | solution.py:20
  137.5 2.3 %copy-start.3 = (bf16[128,2048]{1,0:T(8,128)(2,1)S(1)}, bf16[128,2048]{1,0:T(8,128)(2,1)}, u32[]{:S(2)}) copy-start(bf16[128,2048]{1,0:T(8,128)(2,1)} %get-tuple-element.21) | copy-start | bytes 1572868

commit v2 on v1

v2 whole, which is shorter than its diff:
```python
import functools

import jax
import jax.numpy as jnp
from jax import lax
from jax.experimental import pallas as pl
from jax.experimental.pallas import tpu as pltpu
from jax.sharding import PartitionSpec as P

epsilon = 1e-06
halo_depth = 16
MESH = pl.DeviceIdType.MESH
bf16 = jnp.bfloat16
f32 = jnp.float32


def kernel(
    n, n_ep, cap, top, chunks,
    x_ref, gain_ref, routes_ref, pool_ref, map_ref, scale_ref, gate_hbm, up_hbm, down_hbm, out_w_hbm,
    pool_out, expert_out,
    wg, wu, wd, wo, tok, meta, pools, packed, rows, back, gates, ups, hidden,
    part, from_left, from_right, acc, halo, extended,
    w_sem, halo_send, halo_recv, tok_recv, tok_right, tok_left, meta_recv, meta_right, meta_left,
    pool_recv, pool_right, pool_left, pk_send, pk_recv, bk_send, bk_recv,
    rs_right, rs_right_recv, rs_left, rs_left_recv,
):
    me = lax.axis_index("tp")
    mine = lax.axis_index("ep")
    tokens, width = x_ref.shape
    slots = n_ep * cap
    d_expert = wg.shape[1]
    row_count, shard = pool_ref.shape
    group_dim = map_ref.shape[1]
    groups_local = shard // group_dim
    wc = width // chunks
    has_left, has_right = me > 0, me < n - 1

    def peer(q):
        return lax.rem(mine + q, n_ep)

    def at_slots(p):
        return pl.ds(pl.multiple_of(p * cap, cap), cap)

    def at_chunk(c):
        return pl.ds(pl.multiple_of(c * wc, wc), wc)

    def each(count, body):
        def run(i, _):
            body(i)
            return 0

        lax.fori_loop(0, count, run, 0)

    loads = [
        pltpu.make_async_copy(src, dst, w_sem.at[i])
        for i, (src, dst) in enumerate(
            ((gate_hbm.at[0], wg), (up_hbm.at[0], wu), (down_hbm.at[0], wd), (out_w_hbm, wo))
        )
    ]
    for load in loads:
        load.start()

    barrier = pltpu.get_barrier_semaphore()

    @pl.when(has_left)
    def _():
        pl.semaphore_signal(barrier, inc=1, device_id={"tp": me - 1}, device_id_type=MESH)

    @pl.when(has_right)
    def _():
        pl.semaphore_signal(barrier, inc=1, device_id={"tp": me + 1}, device_id_type=MESH)

    for q in range(1, n_ep):
        pl.semaphore_signal(barrier, inc=1, device_id={"ep": peer(q)}, device_id_type=MESH)

    experts = n * n_ep
    number = lax.broadcasted_iota(jnp.int32, (experts, tokens), 0)
    base = (lax.rem(number, n) * slots + lax.div(number, n) * cap).astype(f32)
    number = number.astype(f32)
    upper = jnp.where(
        lax.broadcasted_iota(jnp.int32, (tokens, tokens), 0)
        < lax.broadcasted_iota(jnp.int32, (tokens, tokens), 1),
        1.0, 0.0,
    ).astype(bf16)
    used = jnp.zeros((experts, 1), f32)
    for k in range(top):
        hot = jnp.where(number == routes_ref[k : k + 1, :], 1.0, 0.0)
        before = jnp.dot(hot.astype(bf16), upper, preferred_element_type=f32) + used
        meta[me, k : k + 1, :] = jnp.sum((base + before) * hot, axis=0, keepdims=True)
        meta[me, top + k : top + k + 1, :] = routes_ref[top + k : top + k + 1, :]
        used = used + jnp.sum(hot, axis=1, keepdims=True)

    tile_t = 32

    def norm(i):
        at = pl.ds(pl.multiple_of(i * tile_t, tile_t), tile_t)
        held = x_ref[at, :].astype(f32)
        held = held * lax.rsqrt(jnp.mean(held * held, axis=1, keepdims=True) + epsilon)
        held = (held * gain_ref[...]).astype(bf16)
        for c in range(chunks):
            tok[me, c, at, :] = held[:, c * wc : (c + 1) * wc]

    each(tokens // tile_t, norm)

    neighbours = jnp.where(has_left, 1, 0) + jnp.where(has_right, 1, 0)
    pl.semaphore_wait(barrier, n_ep - 1 + neighbours)

    def source(j):
        least = jnp.minimum(me, n - 1 - me)
        k = (j + 1) // 2
        near = jnp.where(j % 2 == 1, me - k, me + k)
        k_far = j - least
        far = jnp.where(me > n - 1 - me, me - k_far, me + k_far)
        return jnp.where(j <= 2 * least, near, far)

    def hop(src, dst, where, send, recv, step):
        return pltpu.make_async_remote_copy(
            src_ref=src.at[where], dst_ref=dst.at[where],
            send_sem=send.at[where], recv_sem=recv.at[where],
            device_id={"tp": me + step}, device_id_type=MESH,
        )

    token_lane = (tok, tok_right, tok_left, tok_recv)
    meta_lane = (meta, meta_right, meta_left, meta_recv)
    pool_lane = (pools, pool_right, pool_left, pool_recv)

    def pass_on(lane, s, where):
        buffer, right, left, recv = lane

        @pl.when((s <= me) & has_right)
        def _():
            hop(buffer, buffer, where, right, recv, 1).start()

        @pl.when((s >= me) & has_left)
        def _():
            hop(buffer, buffer, where, left, recv, -1).start()

    def arrive(lane, where):
        buffer, right, left, recv = lane
        hop(buffer, buffer, where, right, recv, 1).wait_recv()

    def passed(lane, s, where):
        buffer, right, left, recv = lane

        @pl.when((s <= me) & has_right)
        def _():
            hop(buffer, buffer, where, right, recv, 1).wait_send()

        @pl.when((s >= me) & has_left)
        def _():
            hop(buffer, buffer, where, left, recv, -1).wait_send()

    def exchange(src, dst, s, c, p, send, recv):
        return pltpu.make_async_remote_copy(
            src_ref=src.at[s, c, at_slots(p)], dst_ref=dst.at[s, c, at_slots(mine)],
            send_sem=send.at[s, c, p], recv_sem=recv.at[s, c, mine],
            device_id={"ep": p}, device_id_type=MESH,
        )

    def exchanged(dst, s, c, p, send, recv):
        return pltpu.make_async_remote_copy(
            src_ref=dst.at[s, c, at_slots(p)], dst_ref=dst.at[s, c, at_slots(p)],
            send_sem=send.at[s, c, p], recv_sem=recv.at[s, c, p],
            device_id={"ep": p}, device_id_type=MESH,
        )

    def slot_masks(s, use_weight):
        row = lax.broadcasted_iota(jnp.int32, (slots, tokens), 0) + me * slots
        row = row.astype(f32)
        held = meta[s]
        total = jnp.zeros((slots, tokens), f32)
        for k in range(top):
            value = held[top + k : top + k + 1] if use_weight else 1.0
            total = total + jnp.where(row == held[k : k + 1], value, 0.0)
        return total

    tile_h = min(256, d_expert)
    tile_r = min(256, row_count)

    def at_h(i):
        return pl.ds(pl.multiple_of(i * tile_h, tile_h), tile_h)

    def at_r(i):
        return pl.ds(pl.multiple_of(i * tile_r, tile_r), tile_r)

    def dispatch(j):
        s = source(j)

        @pl.when(j > 0)
        def _():
            arrive(meta_lane, (s,))
            pass_on(meta_lane, s, (s,))

        choose = slot_masks(s, False).astype(bf16)

        def chunk(c):
            @pl.when(j > 0)
            def _():
                arrive(token_lane, (s, c))
                pass_on(token_lane, s, (s, c))

            packed[s, c] = jnp.dot(choose, tok[s, c], preferred_element_type=f32).astype(bf16)
            for q in range(1, n_ep):
                exchange(packed, rows, s, c, peer(q), pk_send, pk_recv).start()
            rows[s, c, at_slots(mine)] = packed[s, c, at_slots(mine)]

        each(chunks, chunk)

        @pl.when((s == 0) & has_right)
        def _():
            hop(pools, pools, (me,), pool_right, pool_recv, 1).start()

        @pl.when((s == n - 1) & has_left)
        def _():
            hop(pools, pools, (me,), pool_left, pool_recv, -1).start()

    def expert(s):
        def gather(c):
            for q in range(1, n_ep):
                exchanged(rows, s, c, peer(q), pk_send, pk_recv).wait_recv()

            def inner(i):
                here = rows[s, c]
                gate = jnp.dot(here, wg[at_chunk(c), at_h(i)], preferred_element_type=f32)
                up = jnp.dot(here, wu[at_chunk(c), at_h(i)], preferred_element_type=f32)

                @pl.when(c == 0)
                def _():
                    gates[:, at_h(i)] = gate
                    ups[:, at_h(i)] = up

                @pl.when(c > 0)
                def _():
                    gates[:, at_h(i)] += gate
                    ups[:, at_h(i)] += up

            each(d_expert // tile_h, inner)

        each(chunks, gather)
        gate = gates[...]
        hidden[...] = (gate / (1.0 + jnp.exp(-gate)) * ups[...]).astype(bf16)

        def outer(c):
            rows[s, c] = jnp.dot(
                hidden[...], wd[:, at_chunk(c)], preferred_element_type=f32
            ).astype(bf16)
            for q in range(1, n_ep):
                exchange(rows, back, s, c, peer(q), bk_send, bk_recv).start()
            back[s, c, at_slots(mine)] = rows[s, c, at_slots(mine)]

        each(chunks, outer)

    def combine(s):
        weights = slot_masks(s, True)
        high = weights.astype(bf16)
        low = (weights - high.astype(f32)).astype(bf16)
        dims = (((0,), (0,)), ((), ()))

        def chunk(c):
            for q in range(1, n_ep):
                exchanged(back, s, c, peer(q), bk_send, bk_recv).wait_recv()
            here = back[s, c]
            part[s, c] = (
                lax.dot_general(high, here, dims, preferred_element_type=f32)
                + lax.dot_general(low, here, dims, preferred_element_type=f32)
            ).astype(bf16)

            @pl.when((me == 0) & (s > me))
            def _():
                hop(part, from_left, (s, c), rs_right, rs_right_recv, 1).start()

            @pl.when((me == n - 1) & (s < me))
            def _():
                hop(part, from_right, (s, c), rs_left, rs_left_recv, -1).start()

        each(chunks, chunk)

    def project(s, first):
        def tile(i):
            product = jnp.dot(
                pools[s, at_r(i), :], wo[pl.ds(pl.multiple_of(s * shard, shard), shard), :],
                preferred_element_type=f32,
            )
            acc[at_r(i), :] = product if first else acc[at_r(i), :] + product

        each(row_count // tile_r, tile)

    pass_on(meta_lane, me, (me,))
    each(chunks, lambda c: pass_on(token_lane, me, (me, c)))

    def halo_hop():
        return pltpu.make_async_remote_copy(
            src_ref=pool_ref.at[pl.ds(row_count - halo_depth, halo_depth)], dst_ref=halo,
            send_sem=halo_send.at[0], recv_sem=halo_recv.at[0],
            device_id={"ep": lax.rem(mine + 1, n_ep)}, device_id_type=MESH,
        )

    @pl.when(mine < n_ep - 1)
    def _():
        halo_hop().start()

    def widen(i):
        at = pl.ds(pl.multiple_of(i * tile_r + halo_depth, 16), tile_r)
        extended[at, :] = pool_ref[at_r(i), :].astype(f32)

    each(row_count // tile_r, widen)

    @pl.when(mine == 0)
    def _():
        extended[0:halo_depth, :] = jnp.zeros((halo_depth, shard), f32)

    @pl.when(mine > 0)
    def _():
        halo_hop().wait_recv()
        extended[0:halo_depth, :] = halo[...].astype(f32)

    tile_p = min(128, row_count)

    def pooling(i):
        start = pl.multiple_of(i * tile_p, tile_p)
        for g in range(groups_local):
            group = me * groups_local + g
            turn = lax.rem(group, 4)
            lanes = slice(g * group_dim, (g + 1) * group_dim)
            held = extended[pl.ds(start, tile_p + halo_depth), lanes]
            two = held[1:] + held[:-1]
            four = two[2:] + two[:-2]
            eight = four[4:] + four[:-4]
            sixteen = eight[8:] + eight[:-8]
            summed = jnp.where(
                turn == 0, two[15:],
                jnp.where(turn == 1, four[13:], jnp.where(turn == 2, eight[9:], sixteen[1:])),
            )
            window = jnp.where(
                turn == 0, 2, jnp.where(turn == 1, 4, jnp.where(turn == 2, 8, 16))
            )
            place = lax.broadcasted_iota(jnp.int32, (tile_p, group_dim), 0)
            place = place + (mine * row_count + start + 1)
            counted = jnp.minimum(place, window).astype(f32)
            pooled = (summed / counted - held[halo_depth:]).astype(bf16)
            mapped = jnp.dot(pooled, map_ref[group], preferred_element_type=f32)
            pools[me, pl.ds(start, tile_p), lanes] = (mapped * scale_ref[group]).astype(bf16)

    each(row_count // tile_p, pooling)
    loads[3].wait()
    project(me, True)

    def step(j):
        @pl.when(j < n)
        def _():
            dispatch(j)

        @pl.when(j == 1)
        def _():
            for load in loads[:3]:
                load.wait()

        @pl.when((j >= 1) & (j <= n))
        def _():
            expert(source(j - 1))

        @pl.when(j >= 2)
        def _():
            combine(source(j - 2))

    each(n + 2, step)

    def add_on(buffer, d, send, recv, to):
        def chunk(c):
            hop(part, buffer, (d, c), send, recv, to).wait_recv()
            buffer[d, c] = (buffer[d, c].astype(f32) + part[d, c].astype(f32)).astype(bf16)
            hop(buffer, buffer, (d, c), send, recv, to).start()

        each(chunks, chunk)

    def tail(i):
        s = source(i + 1)
        arrive(pool_lane, (s,))
        pass_on(pool_lane, s, (s,))
        project(s, False)
        right, left = i + 1, n - 2 - i

        @pl.when((me > 0) & (me < right))
        def _():
            add_on(from_left, right, rs_right, rs_right_recv, 1)

        @pl.when((me < n - 1) & (me > left))
        def _():
            add_on(from_right, left, rs_left, rs_left_recv, -1)

    each(n - 1, tail)
    pool_out[...] = acc[...].astype(bf16)

    for c in range(chunks):
        columns = slice(c * wc, (c + 1) * wc)

        @pl.when(has_left)
        def _():
            hop(part, from_left, (me, c), rs_right, rs_right_recv, 1).wait_recv()

        @pl.when(has_right)
        def _():
            hop(part, from_right, (me, c), rs_left, rs_left_recv, -1).wait_recv()

        @pl.when(has_left & has_right)
        def _():
            expert_out[:, columns] = (
                part[me, c].astype(f32)
                + from_left[me, c].astype(f32)
                + from_right[me, c].astype(f32)
            ).astype(bf16)

        @pl.when(has_left & jnp.logical_not(has_right))
        def _():
            expert_out[:, columns] = (
                part[me, c].astype(f32) + from_left[me, c].astype(f32)
            ).astype(bf16)

        @pl.when(has_right & jnp.logical_not(has_left))
        def _():
            expert_out[:, columns] = (
                part[me, c].astype(f32) + from_right[me, c].astype(f32)
            ).astype(bf16)

    @pl.when(mine < n_ep - 1)
    def _():
        halo_hop().wait_send()

    def drain(s):
        passed(meta_lane, s, (s,))
        passed(pool_lane, s, (s,))

        def chunk(c):
            passed(token_lane, s, (s, c))
            for q in range(1, n_ep):
                exchange(packed, rows, s, c, peer(q), pk_send, pk_recv).wait_send()
                exchange(rows, back, s, c, peer(q), bk_send, bk_recv).wait_send()

            @pl.when(me < s)
            def _():
                hop(part, from_left, (s, c), rs_right, rs_right_recv, 1).wait_send()

            @pl.when(me > s)
            def _():
                hop(part, from_right, (s, c), rs_left, rs_left_recv, -1).wait_send()

        each(chunks, chunk)

    each(n, drain)


def on_device(
    pool_input, pool_map, pool_scale, out_weight, expert_input, norm_gain,
    routes, route_weight, gate_weight, up_weight, down_weight,
):
    n_ep, n = lax.axis_size("ep"), lax.axis_size("tp")
    tokens, width = expert_input.shape
    top = routes.shape[1]
    cap = max(2 * tokens * top // (n_ep * n), 16)
    slots = n_ep * cap
    chunks = max(1, min(4, 64 // (n_ep * n)))
    wc = width // chunks
    row_count, shard = pool_input.shape
    groups, group_dim = pool_map.shape[:2]
    meta = jnp.concatenate([routes.astype(f32), route_weight.astype(f32)], axis=1).T
    meta = jnp.pad(meta, ((0, -meta.shape[0] % 8), (0, 0)))
    d_expert = gate_weight.shape[2]
    dma = pltpu.SemaphoreType.DMA
    vmem = pl.BlockSpec(memory_space=pltpu.VMEM)
    hbm = pl.BlockSpec(memory_space=pl.ANY)
    one, line, grid, pair = dma((1,)), dma((n,)), dma((n, chunks)), dma((n, chunks, n_ep))
    by_slot = pltpu.VMEM((n, chunks, slots, wc), bf16)
    by_token = pltpu.VMEM((n, chunks, tokens, wc), bf16)
    out_columns = out_weight.shape[1]
    return pl.pallas_call(
        functools.partial(kernel, n, n_ep, cap, top, chunks),
        out_shape=(
            jax.ShapeDtypeStruct((row_count, out_columns), bf16),
            jax.ShapeDtypeStruct((tokens, width), bf16),
        ),
        in_specs=[vmem] * 6 + [hbm] * 4,
        out_specs=(vmem, vmem),
        scratch_shapes=[
            pltpu.VMEM((width, d_expert), bf16),
            pltpu.VMEM((width, d_expert), bf16),
            pltpu.VMEM((d_expert, width), bf16),
            pltpu.VMEM(out_weight.shape, bf16),
            by_token,
            pltpu.VMEM((n,) + meta.shape, f32),
            pltpu.VMEM((n, row_count, shard), bf16),
            by_slot, by_slot, by_slot,
            pltpu.VMEM((slots, d_expert), f32),
            pltpu.VMEM((slots, d_expert), f32),
            pltpu.VMEM((slots, d_expert), bf16),
            by_token, by_token, by_token,
            pltpu.VMEM((row_count, out_columns), f32),
            pltpu.VMEM((halo_depth, shard), bf16),
            pltpu.VMEM((row_count + halo_depth, shard), f32),
            dma((4,)), one, one,
            grid, grid, grid, line, line, line, line, line, line,
            pair, pair, pair, pair,
            grid, grid, grid, grid,
        ],
        compiler_params=pltpu.CompilerParams(
            collective_id=0, has_side_effects=True, vmem_limit_bytes=62 * 1024 * 1024
        ),
    )(
        expert_input, norm_gain.reshape(1, width), meta, pool_input, pool_map,
        pool_scale.reshape(groups, 1, group_dim), gate_weight, up_weight, down_weight, out_weight,
    )


def solution(mesh):
    return jax.shard_map(
        on_device,
        mesh=mesh,
        in_specs=(
            P(("grp", "ep"), "tp"),
            P(),
            P(),
            P(None, "tp"),
            P(("grp", "ep", "tp"), None),
            P(),
            P(("grp", "ep", "tp"), None),
            P(("grp", "ep", "tp"), None),
            P(("ep", "tp"), None, None),
            P(("ep", "tp"), None, None),
            P(("ep", "tp"), None, None),
        ),
        out_specs=(P(("grp", "ep"), "tp"), P(("grp", "ep", "tp"), None)),
        check_vma=False,
    )
```

time: 142 us -> 121 us (0.85); the launches traced: 141 us -> 121 us
  Pallas kernels: 123 us -> 115 us
  other arithmetic: 5.33 us -> 1.37 us
  matrix products: 3.22 us -> 0 us
  local copies, waits for them, and re-layouts: 6.16 us -> 3.72 us
  starting transfers between devices: 2.38 us -> 0 us
    pallas_call x1, Pallas kernels: 123 us -> 115 us  [on_device(): pl.pallas_call(functools.partial(kernel, n, n_ep, cap, top, chunks), out_...]
    dot_general x2 -> x0, matrix products: 3.22 us -> none  [the longest x1 3.01 us: mapped_channels(): jnp.einsum('rgc,gcd->rgd', pooled.reshape(row_count, groups_local, group_...]
    convert_element_type x5 -> x1, other arithmetic: 3.35 us -> 0.68 us  [on_device(): routes.astype(f32)]
    ppermute x1 -> x0, starting transfers between devices: 2.38 us -> none  [shifted_2(): return lax.ppermute(shard, axis, pairs)]
    unnamed x13 -> x4, local copies, waits for them, and re-layouts: 3.93 us -> 3.12 us
  transfers between devices with their start and end apart: 1 -> 0, of which waited for: 0 -> 0; matrix products, arithmetic and copies ran while one was open for 5% -> 0% of each run, Pallas kernels for 0% -> 0%
where the time goes in v2:
time: 121 us
  Pallas kernels  115 us (95%)
  local copies, waits for them, and re-layouts  3.72 us (3%)
  other arithmetic  1.37 us (1%)
    pallas_call x1, Pallas kernels, on_device(): pl.pallas_call(functools.partial(kernel, n, n_ep, cap, top, chunks), out_...  115 us
    unnamed x4, local copies, waits for them, and re-layouts  3.12 us

profile of v2, /device:TPU:0, one launch (start us, length us, event | category | flops | bytes accessed | tf_op | source)
XLA Modules:
  0.0 121.2 jit_solution(14919564048940584879)
XLA Ops:
  0.6 0.7 convert_element_type.5
  1.3 0.7 maximum_bitcast_fusion
  2.0 0.6 pad.4.routes_ref
  2.6 115.4 %shard_map.122 = (bf16[1024,512]{1,0:T(8,128)(2,1)}, bf16[128,2048]{1,0:T(8,128)(2,1)}) custom-call(bf16[128,2048]{1,0:T(8,128)(2,1)} %x_ref.1, f32[1,2048]{1,0:T(1,128)} %bitcast.4, f32[8,128]{1,0:T(8,128)} %pad.4.routes_ref, bf16[1024,256]{1,0:T(8,128)(2,1)} %pool_ref.1, bf16[8,128,128]{2,1,0:T(8,128)(2,1)} %map_ref.1, f32[8,1,128]{2,1,0:T(1,128)} %bitcast.5, ...), custom_call_target="tpu_custom_call" | custom-call | tf_op jit(solution)/shard_map/pallas_call | solution.py:475
  118.0 0.0 copy-start
  118.1 2.3 %copy.15 = bf16[1024,512]{1,0:T(8,128)(2,1)} copy(bf16[1024,512]{1,0:T(8,128)(2,1)} %get-tuple-element.4) | data formatting | bytes 2097152
  120.4 0.0 copy-done
  120.4 0.8 copy.16
Async XLA Ops:
  118.0 2.3 %copy-start = (bf16[128,2048]{1,0:T(8,128)(2,1)S(1)}, bf16[128,2048]{1,0:T(8,128)(2,1)}, u32[]{:S(2)}) copy-start(bf16[128,2048]{1,0:T(8,128)(2,1)} %get-tuple-element.5) | copy-start | bytes 1572868

commit v3 on v2

--- a/solution.py
+++ b/solution.py
@@ -345,48 +345,61 @@
     loads[3].wait()
     project(me, True)
 
-    def step(j):
-        @pl.when(j < n)
-        def _():
-            dispatch(j)
-
-        @pl.when(j == 1)
-        def _():
-            for load in loads[:3]:
-                load.wait()
-
-        @pl.when((j >= 1) & (j <= n))
-        def _():
-            expert(source(j - 1))
-
-        @pl.when(j >= 2)
-        def _():
-            combine(source(j - 2))
-
-    each(n + 2, step)
-
-    def add_on(buffer, d, send, recv, to):
-        def chunk(c):
-            hop(part, buffer, (d, c), send, recv, to).wait_recv()
-            buffer[d, c] = (buffer[d, c].astype(f32) + part[d, c].astype(f32)).astype(bf16)
-            hop(buffer, buffer, (d, c), send, recv, to).start()
-
-        each(chunks, chunk)
-
-    def tail(i):
-        s = source(i + 1)
+    behind = jnp.where(has_left & has_right, 1, 0)
+
+    def take_pool(j):
+        s = source(j)
         arrive(pool_lane, (s,))
         pass_on(pool_lane, s, (s,))
         project(s, False)
+
+    def step(j):
+        at_expert = j - behind
+        at_combine = at_expert - 1
+
+        @pl.when(j < n)
+        def _():
+            dispatch(j)
+
+        @pl.when(at_expert == 0)
+        def _():
+            for load in loads[:3]:
+                load.wait()
+
+        @pl.when((at_combine >= 0) & (at_combine < n))
+        def _():
+            combine(source(at_combine))
+
+        @pl.when((at_expert >= 0) & (at_expert < n))
+        def _():
+            expert(source(at_expert))
+
+    each(n + 2, step)
+
+    def add_on(buffer, d, c, send, recv, to):
+        hop(part, buffer, (d, c), send, recv, to).wait_recv()
+        buffer[d, c] = (buffer[d, c].astype(f32) + part[d, c].astype(f32)).astype(bf16)
+        hop(buffer, buffer, (d, c), send, recv, to).start()
+
+    take_pool(1)
+
+    def tail(i):
         right, left = i + 1, n - 2 - i
 
-        @pl.when((me > 0) & (me < right))
-        def _():
-            add_on(from_left, right, rs_right, rs_right_recv, 1)
-
-        @pl.when((me < n - 1) & (me > left))
-        def _():
-            add_on(from_right, left, rs_left, rs_left_recv, -1)
+        def chunk(c):
+            @pl.when((me > 0) & (me < right))
+            def _():
+                add_on(from_left, right, c, rs_right, rs_right_recv, 1)
+
+            @pl.when((me < n - 1) & (me > left))
+            def _():
+                add_on(from_right, left, c, rs_left, rs_left_recv, -1)
+
+        each(chunks, chunk)
+
+        @pl.when(i + 2 < n)
+        def _():
+            take_pool(i + 2)
 
     each(n - 1, tail)
     pool_out[...] = acc[...].astype(bf16)

time: 121 us -> 133 us (1.099)
  Pallas kernels: 115 us -> 127 us
    pallas_call x1, Pallas kernels: 115 us -> 127 us  [on_device(): pl.pallas_call(functools.partial(kernel, n, n_ep, cap, top, chunks), out_...]
where the time goes in v3:
time: 133 us
  Pallas kernels  127 us (95%)
  local copies, waits for them, and re-layouts  3.72 us (3%)
  other arithmetic  1.37 us (1%)
    pallas_call x1, Pallas kernels, on_device(): pl.pallas_call(functools.partial(kernel, n, n_ep, cap, top, chunks), out_...  127 us
    unnamed x4, local copies, waits for them, and re-layouts  3.12 us

profile of v3, /device:TPU:0, one launch (start us, length us, event | category | flops | bytes accessed | tf_op | source)
XLA Modules:
  0.0 132.5 jit_solution(1193557443731347743)
XLA Ops:
  0.6 0.7 convert_element_type.5
  1.3 0.7 maximum_bitcast_fusion
  2.0 0.6 pad.4.routes_ref
  2.6 126.8 %shard_map.122 = (bf16[1024,512]{1,0:T(8,128)(2,1)}, bf16[128,2048]{1,0:T(8,128)(2,1)}) custom-call(bf16[128,2048]{1,0:T(8,128)(2,1)} %x_ref.1, f32[1,2048]{1,0:T(1,128)} %bitcast.4, f32[8,128]{1,0:T(8,128)} %pad.4.routes_ref, bf16[1024,256]{1,0:T(8,128)(2,1)} %pool_ref.1, bf16[8,128,128]{2,1,0:T(8,128)(2,1)} %map_ref.1, f32[8,1,128]{2,1,0:T(1,128)} %bitcast.5, ...), custom_call_target="tpu_custom_call" | custom-call | tf_op jit(solution)/shard_map/pallas_call | solution.py:488
  129.4 0.0 copy-start
  129.4 2.3 %copy.15 = bf16[1024,512]{1,0:T(8,128)(2,1)} copy(bf16[1024,512]{1,0:T(8,128)(2,1)} %get-tuple-element.4) | data formatting | bytes 2097152
  131.7 0.0 copy-done
  131.7 0.8 copy.16
Async XLA Ops:
  129.4 2.3 %copy-start = (bf16[128,2048]{1,0:T(8,128)(2,1)S(1)}, bf16[128,2048]{1,0:T(8,128)(2,1)}, u32[]{:S(2)}) copy-start(bf16[128,2048]{1,0:T(8,128)(2,1)} %get-tuple-element.5) | copy-start | bytes 1572868
